TPU v7x, 128 devices: a whole 4x4x4 slice. The times are simulated.
128 devices in a mesh: sp: 16 (over z, x), dp: 8 (over y, core).
Axes of the slice: x: 4, y: 4, z: 4, core: 2. Of those that a mesh axis runs over, the one named last changes fastest.
Arguments:
- tokens: bfloat16 [8, 6144, 2048], P('dp', 'sp'), may hold values from -6 to 6
- q_weight: bfloat16 [2048, 1024], P(('sp', 'dp')), may hold values from -0.13258252 to 0.13258252
- k_weight: bfloat16 [2048, 256], P(('sp', 'dp')), may hold values from -0.13258252 to 0.13258252
- v_weight: bfloat16 [2048, 256], P(('sp', 'dp')), may hold values from -0.125 to 0.125
- out_weight: bfloat16 [1024, 2048], P(None, ('sp', 'dp')), may hold values from -6 to 6
- q_gain: float32 [64], replicated, may hold values from 0.5 to 8
- k_gain: float32 [64], replicated, may hold values from 0.5 to 8
Outputs:
- mixed: bfloat16 [8, 6144, 2048], P('dp', 'sp')
All inputs are finite; a program needn't handle non-finite values.
Results may differ from a plain program's by a relative error of at most 0.0055.
The roundings to bfloat16 on the way count: a program that leaves them out, or rounds other values in their place, can miss the bound.
Values may be sent and summed in bfloat16 or wider, within the bound.
No kernel may reach another device: no remote copies, remote signals or barrier semaphores. Data moves between devices by JAX's collectives and lax.ppermute only.
A program may use at most 128 MiB of HBM per device.

v0:
```python
import math

import jax
import jax.numpy as jnp
from jax import lax
from jax.sharding import PartitionSpec as P

GRID_W = 64


epsilon = 1e-06
rope_base = 10000.0


def in_one_piece(arrays, axis, dim, along):
    widths = [a.shape[along] for a in arrays]
    both = jnp.concatenate(arrays, axis=along)
    filled = lax.all_gather(both, axis, axis=dim, tiled=True)
    return tuple(jnp.split(filled, [sum(widths[:k]) for k in range(1, len(widths))], axis=along))


def normalize(tensor, gain_vec):
    mean_sq = jnp.mean(tensor * tensor, axis=-1, keepdims=True)
    return tensor * lax.rsqrt(mean_sq + epsilon) * gain_vec


def rotate(tensor, offset):
    row_count = tensor.shape[0]
    head_width = tensor.shape[2]
    quarter = head_width // 4
    half_width = head_width // 2
    positions = jnp.arange(row_count, dtype=jnp.int32) + offset
    frequency = rope_base ** (-jnp.arange(quarter, dtype=jnp.float32) / quarter)

    def rotate_pair(segment, coords):
        angles = coords.astype(jnp.float32)[:, None] * frequency[None, :]
        cosine = jnp.cos(angles)[:, None, :]
        sine_val = jnp.sin(angles)[:, None, :]
        low_half = segment[..., :quarter]
        high_half = segment[..., quarter:]
        return jnp.concatenate(
            [low_half * cosine - high_half * sine_val, high_half * cosine + low_half * sine_val],
            axis=-1,
        )

    return jnp.concatenate(
        [
            rotate_pair(tensor[..., :half_width], positions // GRID_W),
            rotate_pair(tensor[..., half_width:], positions % GRID_W),
        ],
        axis=-1,
    )


def attend(query_rows, key_rows, value_rows):
    row_count, head_width = query_rows.shape
    block_rows = math.gcd(row_count, 512)
    score_scale = head_width ** (-0.5)

    def attend_block(segment):
        scores = (
            lax.dot_general(
                segment, key_rows, (((1,), (1,)), ((), ())), preferred_element_type=jnp.float32
            )
            * score_scale
        )
        row_max = jnp.max(scores, axis=-1, keepdims=True)
        weights = jnp.exp(scores - row_max)
        shares = (weights / jnp.sum(weights, axis=-1, keepdims=True)).astype(jnp.bfloat16)
        return jnp.dot(shares, value_rows, preferred_element_type=jnp.float32).astype(jnp.bfloat16)

    blocks = query_rows.reshape(row_count // block_rows, block_rows, head_width)
    return lax.map(attend_block, blocks).reshape(row_count, head_width)


def per_device(tokens, q_weight, k_weight, v_weight, out_weight, q_gain, k_gain):
    rows_in = tokens[0]
    tok_count = rows_in.shape[0]
    head_width = q_gain.shape[0]
    q_width = out_weight.shape[0]
    kv_width = k_weight.shape[1]
    q_heads = q_width // head_width
    kv_heads = kv_width // head_width
    group_size = q_heads // kv_heads
    offset = lax.axis_index("sp") * tok_count
    weight_rows = in_one_piece((q_weight, k_weight, v_weight), ("sp", "dp"), 0, 1)
    query_raw, key_raw, value_raw = tuple(
        (
            jnp.dot(rows_in, rows_part, preferred_element_type=jnp.float32)
            for rows_part in weight_rows
        )
    )
    queries = rotate(
        normalize(query_raw.reshape(tok_count, q_heads, head_width), q_gain), offset
    ).astype(jnp.bfloat16)
    keys_rot = rotate(
        normalize(key_raw.reshape(tok_count, kv_heads, head_width), k_gain), offset
    ).astype(jnp.bfloat16)
    values_dev = value_raw.astype(jnp.bfloat16)
    keys_wide = jnp.broadcast_to(
        keys_rot[:, :, None, :], (tok_count, kv_heads, group_size, head_width)
    ).reshape(tok_count, q_width)
    values_wide = jnp.broadcast_to(
        values_dev.reshape(tok_count, kv_heads, 1, head_width),
        (tok_count, kv_heads, group_size, head_width),
    ).reshape(tok_count, q_width)
    q_local, k_local, v_local = (
        lax.all_to_all(
            queries.reshape(tok_count, q_width), "sp", split_axis=1, concat_axis=0, tiled=True
        ),
        lax.all_to_all(keys_wide, "sp", split_axis=1, concat_axis=0, tiled=True),
        lax.all_to_all(values_wide, "sp", split_axis=1, concat_axis=0, tiled=True),
    )
    outputs = attend(q_local, k_local, v_local)
    attended = lax.all_to_all(outputs, "sp", split_axis=0, concat_axis=1, tiled=True)
    result = jnp.dot(
        attended,
        lax.all_gather(out_weight, ("sp", "dp"), axis=1, tiled=True),
        preferred_element_type=jnp.float32,
    ).astype(jnp.bfloat16)
    return result[None]


def solution(mesh):
    return jax.shard_map(
        per_device,
        mesh=mesh,
        in_specs=(
            P("dp", "sp", None),
            P(("sp", "dp"), None),
            P(("sp", "dp"), None),
            P(("sp", "dp"), None),
            P(None, ("sp", "dp")),
            P(),
            P(),
        ),
        out_specs=P("dp", "sp", None),
        check_vma=False,
    )
```

profile of v0, /device:TPU:0, one launch (start us, length us, event | category | flops | bytes accessed | tf_op | source)
XLA Modules:
  0.0 280.0 jit_solution(8570700973020452370)
XLA Ops:
  8.4 72.8 %all-gather.3.cloned.1.call-done = bf16[2048,1536]{1,0:T(8,128)(2,1)} async-done(((bf16[16,1536]{1,0:T(8,128)(2,1)}), bf16[2048,1536]{1,0:T(8,128)(2,1)}) %all-gather.3.cloned.1.call-update) | async-done | bytes 6291472 | tf_op jit(solution)/shard_map/all_gather | solution.py:18
  84.4 4.4 %all-to-all-start.1 = ((bf16[384,16,64]{0,2,1:T(8,128)(2,1)}), bf16[384,16,64]{0,2,1:T(8,128)(2,1)S(1)}, u32[]{:S(2)}, u32[]{:S(2)}) async-start(bf16[384,16,64]{0,2,1:T(8,128)(2,1)} %bitcast.11), calls=%async_computation.1 | async-start | bytes 1572864 | tf_op jit(solution)/shard_map/all_to_all | solution.py:111
  88.8 4.6 %multiply_reduce_fusion.1 = (f32[384,16]{0,1:T(8,128)S(1)}, f32[1024,384]{1,0:T(8,128)S(1)}) fusion(bf16[1,384,2048]{2,1,0:T(8,128)(2,1)S(1)} %copy-done, bf16[2048,1536]{1,0:T(8,128)(2,1)} %all-gather.3.cloned.1.call-done), kind=kOutput, calls=%fused_computation.23 | convolution fusion | flops 1611393024 | bytes 7364608 | tf_op jit(solution)/shard_map/dot_general | solution.py:89
  95.0 8.5 %all-to-all-done.1 = bf16[384,16,64]{0,2,1:T(8,128)(2,1)S(1)} async-done(((bf16[384,16,64]{0,2,1:T(8,128)(2,1)}), bf16[384,16,64]{0,2,1:T(8,128)(2,1)S(1)}, u32[]{:S(2)}, u32[]{:S(2)}) %all-to-all-start.1) | async-done | bytes 786464 | tf_op jit(solution)/shard_map/all_to_all | solution.py:111
  103.5 3.6 %all-to-all-start = ((bf16[384,16,64]{0,2,1:T(8,128)(2,1)}), bf16[384,16,64]{0,2,1:T(8,128)(2,1)S(1)}, u32[]{:S(2)}, u32[]{:S(2)}) async-start(bf16[384,16,64]{0,2,1:T(8,128)(2,1)} %pad_maximum_fusion), calls=%async_computation | async-start | bytes 1572864 | tf_op jit(solution)/shard_map/all_to_all | solution.py:108
  109.1 11.7 %all-to-all-done = bf16[384,16,64]{0,2,1:T(8,128)(2,1)S(1)} async-done(((bf16[384,16,64]{0,2,1:T(8,128)(2,1)}), bf16[384,16,64]{0,2,1:T(8,128)(2,1)S(1)}, u32[]{:S(2)}, u32[]{:S(2)}) %all-to-all-start) | async-done | bytes 786464 | tf_op jit(solution)/shard_map/all_to_all | solution.py:108
  121.9 4.3 %all-to-all-start.2 = ((bf16[384,16,64]{0,2,1:T(8,128)(2,1)}), bf16[384,16,64]{0,2,1:T(8,128)(2,1)}, u32[]{:S(2)}, u32[]{:S(2)}) async-start(bf16[384,16,64]{0,2,1:T(8,128)(2,1)} %bitcast.16), calls=%async_computation.2 | async-start | bytes 1572864 | tf_op jit(solution)/shard_map/all_to_all | solution.py:112
  131.2 7.8 %all-to-all-done.2 = bf16[384,16,64]{0,2,1:T(8,128)(2,1)} async-done(((bf16[384,16,64]{0,2,1:T(8,128)(2,1)}), bf16[384,16,64]{0,2,1:T(8,128)(2,1)}, u32[]{:S(2)}, u32[]{:S(2)}) %all-to-all-start.2) | async-done | bytes 786464 | tf_op jit(solution)/shard_map/all_to_all | solution.py:112
  141.5 107.6 %while.10 = (s32[]{:T(128)}, bf16[12,512,64]{1,2,0:T(8,128)(2,1)}, bf16[12,512,64]{2,1,0:T(8,128)(2,1)}, bf16[6144,64]{1,0:T(8,128)(2,1)S(1)}, bf16[6144,64]{1,0:T(8,128)(2,1)}, /*index=5*/s32[]{:T(128)}) while((s32[]{:T(128)}, bf16[12,512,64]{1,2,0:T(8,128)(2,1)}, bf16[12,512,64]{2,1,0:T(8,128)(2,1)}, bf16[6144,64]{1,0:T(8,128)(2,1)S(1)}, ...), condition=%wide.region_5.6_spmd, body=%wide.region_2.5_spmd.sunk | while | flops 833649664 | bytes 42675296 | solution.py:73
  141.5 2.8 multiply_reduce_fusion.4
  146.5 4.0 %fusion.39 = bf16[12,512,64]{1,2,0:T(8,128)(2,1)} fusion(bf16[12,512,64]{1,2,0:T(8,128)(2,1)} %get-tuple-element.116, s32[]{:T(128)} %get-tuple-element.115, bf16[6144,64]{1,0:T(8,128)(2,1)S(1)} %copy-done.3, f32[512,6144]{1,0:T(8,128)S(1)} %get-tuple-element.107, f32[512]{0:T(512)S(1)} %fusion.38, f32[512]{0:T(512)S(1)} %get-tuple-element.108), kind=kOutput, calls=%fused_computation.7.clone.1 | convolution fusion | flops 415268864 | bytes 13439488 | tf_op jit(solution)/shard_map/while/body/eval_jaxpr/dot_general | solution.py:70
  150.5 2.8 multiply_reduce_fusion.4
  155.5 4.0 %fusion.39 = bf16[12,512,64]{1,2,0:T(8,128)(2,1)} fusion(bf16[12,512,64]{1,2,0:T(8,128)(2,1)} %get-tuple-element.116, s32[]{:T(128)} %get-tuple-element.115, bf16[6144,64]{1,0:T(8,128)(2,1)S(1)} %copy-done.3, f32[512,6144]{1,0:T(8,128)S(1)} %get-tuple-element.107, f32[512]{0:T(512)S(1)} %fusion.38, f32[512]{0:T(512)S(1)} %get-tuple-element.108), kind=kOutput, calls=%fused_computation.7.clone.1 | convolution fusion | flops 415268864 | bytes 13439488 | tf_op jit(solution)/shard_map/while/body/eval_jaxpr/dot_general | solution.py:70
  159.4 2.8 multiply_reduce_fusion.4
  164.4 4.0 %fusion.39 = bf16[12,512,64]{1,2,0:T(8,128)(2,1)} fusion(bf16[12,512,64]{1,2,0:T(8,128)(2,1)} %get-tuple-element.116, s32[]{:T(128)} %get-tuple-element.115, bf16[6144,64]{1,0:T(8,128)(2,1)S(1)} %copy-done.3, f32[512,6144]{1,0:T(8,128)S(1)} %get-tuple-element.107, f32[512]{0:T(512)S(1)} %fusion.38, f32[512]{0:T(512)S(1)} %get-tuple-element.108), kind=kOutput, calls=%fused_computation.7.clone.1 | convolution fusion | flops 415268864 | bytes 13439488 | tf_op jit(solution)/shard_map/while/body/eval_jaxpr/dot_general | solution.py:70
  168.4 2.8 multiply_reduce_fusion.4
  173.4 4.0 %fusion.39 = bf16[12,512,64]{1,2,0:T(8,128)(2,1)} fusion(bf16[12,512,64]{1,2,0:T(8,128)(2,1)} %get-tuple-element.116, s32[]{:T(128)} %get-tuple-element.115, bf16[6144,64]{1,0:T(8,128)(2,1)S(1)} %copy-done.3, f32[512,6144]{1,0:T(8,128)S(1)} %get-tuple-element.107, f32[512]{0:T(512)S(1)} %fusion.38, f32[512]{0:T(512)S(1)} %get-tuple-element.108), kind=kOutput, calls=%fused_computation.7.clone.1 | convolution fusion | flops 415268864 | bytes 13439488 | tf_op jit(solution)/shard_map/while/body/eval_jaxpr/dot_general | solution.py:70
  177.4 2.8 multiply_reduce_fusion.4
  182.4 4.0 %fusion.39 = bf16[12,512,64]{1,2,0:T(8,128)(2,1)} fusion(bf16[12,512,64]{1,2,0:T(8,128)(2,1)} %get-tuple-element.116, s32[]{:T(128)} %get-tuple-element.115, bf16[6144,64]{1,0:T(8,128)(2,1)S(1)} %copy-done.3, f32[512,6144]{1,0:T(8,128)S(1)} %get-tuple-element.107, f32[512]{0:T(512)S(1)} %fusion.38, f32[512]{0:T(512)S(1)} %get-tuple-element.108), kind=kOutput, calls=%fused_computation.7.clone.1 | convolution fusion | flops 415268864 | bytes 13439488 | tf_op jit(solution)/shard_map/while/body/eval_jaxpr/dot_general | solution.py:70
  186.3 2.8 multiply_reduce_fusion.4
  191.3 4.0 %fusion.39 = bf16[12,512,64]{1,2,0:T(8,128)(2,1)} fusion(bf16[12,512,64]{1,2,0:T(8,128)(2,1)} %get-tuple-element.116, s32[]{:T(128)} %get-tuple-element.115, bf16[6144,64]{1,0:T(8,128)(2,1)S(1)} %copy-done.3, f32[512,6144]{1,0:T(8,128)S(1)} %get-tuple-element.107, f32[512]{0:T(512)S(1)} %fusion.38, f32[512]{0:T(512)S(1)} %get-tuple-element.108), kind=kOutput, calls=%fused_computation.7.clone.1 | convolution fusion | flops 415268864 | bytes 13439488 | tf_op jit(solution)/shard_map/while/body/eval_jaxpr/dot_general | solution.py:70
  195.3 2.8 multiply_reduce_fusion.4
  200.3 4.0 %fusion.39 = bf16[12,512,64]{1,2,0:T(8,128)(2,1)} fusion(bf16[12,512,64]{1,2,0:T(8,128)(2,1)} %get-tuple-element.116, s32[]{:T(128)} %get-tuple-element.115, bf16[6144,64]{1,0:T(8,128)(2,1)S(1)} %copy-done.3, f32[512,6144]{1,0:T(8,128)S(1)} %get-tuple-element.107, f32[512]{0:T(512)S(1)} %fusion.38, f32[512]{0:T(512)S(1)} %get-tuple-element.108), kind=kOutput, calls=%fused_computation.7.clone.1 | convolution fusion | flops 415268864 | bytes 13439488 | tf_op jit(solution)/shard_map/while/body/eval_jaxpr/dot_general | solution.py:70
  209.2 4.0 %fusion.39 = bf16[12,512,64]{1,2,0:T(8,128)(2,1)} fusion(bf16[12,512,64]{1,2,0:T(8,128)(2,1)} %get-tuple-element.116, s32[]{:T(128)} %get-tuple-element.115, bf16[6144,64]{1,0:T(8,128)(2,1)S(1)} %copy-done.3, f32[512,6144]{1,0:T(8,128)S(1)} %get-tuple-element.107, f32[512]{0:T(512)S(1)} %fusion.38, f32[512]{0:T(512)S(1)} %get-tuple-element.108), kind=kOutput, calls=%fused_computation.7.clone.1 | convolution fusion | flops 415268864 | bytes 13439488 | tf_op jit(solution)/shard_map/while/body/eval_jaxpr/dot_general | solution.py:70
  218.2 4.0 %fusion.39 = bf16[12,512,64]{1,2,0:T(8,128)(2,1)} fusion(bf16[12,512,64]{1,2,0:T(8,128)(2,1)} %get-tuple-element.116, s32[]{:T(128)} %get-tuple-element.115, bf16[6144,64]{1,0:T(8,128)(2,1)S(1)} %copy-done.3, f32[512,6144]{1,0:T(8,128)S(1)} %get-tuple-element.107, f32[512]{0:T(512)S(1)} %fusion.38, f32[512]{0:T(512)S(1)} %get-tuple-element.108), kind=kOutput, calls=%fused_computation.7.clone.1 | convolution fusion | flops 415268864 | bytes 13439488 | tf_op jit(solution)/shard_map/while/body/eval_jaxpr/dot_general | solution.py:70
  227.2 4.0 %fusion.39 = bf16[12,512,64]{1,2,0:T(8,128)(2,1)} fusion(bf16[12,512,64]{1,2,0:T(8,128)(2,1)} %get-tuple-element.116, s32[]{:T(128)} %get-tuple-element.115, bf16[6144,64]{1,0:T(8,128)(2,1)S(1)} %copy-done.3, f32[512,6144]{1,0:T(8,128)S(1)} %get-tuple-element.107, f32[512]{0:T(512)S(1)} %fusion.38, f32[512]{0:T(512)S(1)} %get-tuple-element.108), kind=kOutput, calls=%fused_computation.7.clone.1 | convolution fusion | flops 415268864 | bytes 13439488 | tf_op jit(solution)/shard_map/while/body/eval_jaxpr/dot_general | solution.py:70
  236.1 4.0 %fusion.39 = bf16[12,512,64]{1,2,0:T(8,128)(2,1)} fusion(bf16[12,512,64]{1,2,0:T(8,128)(2,1)} %get-tuple-element.116, s32[]{:T(128)} %get-tuple-element.115, bf16[6144,64]{1,0:T(8,128)(2,1)S(1)} %copy-done.3, f32[512,6144]{1,0:T(8,128)S(1)} %get-tuple-element.107, f32[512]{0:T(512)S(1)} %fusion.38, f32[512]{0:T(512)S(1)} %get-tuple-element.108), kind=kOutput, calls=%fused_computation.7.clone.1 | convolution fusion | flops 415268864 | bytes 13439488 | tf_op jit(solution)/shard_map/while/body/eval_jaxpr/dot_general | solution.py:70
  240.1 2.8 multiply_reduce_fusion.4
  245.1 4.0 %fusion.39 = bf16[12,512,64]{1,2,0:T(8,128)(2,1)} fusion(bf16[12,512,64]{1,2,0:T(8,128)(2,1)} %get-tuple-element.116, s32[]{:T(128)} %get-tuple-element.115, bf16[6144,64]{1,0:T(8,128)(2,1)S(1)} %copy-done.3, f32[512,6144]{1,0:T(8,128)S(1)} %get-tuple-element.107, f32[512]{0:T(512)S(1)} %fusion.38, f32[512]{0:T(512)S(1)} %get-tuple-element.108), kind=kOutput, calls=%fused_computation.7.clone.1 | convolution fusion | flops 415268864 | bytes 13439488 | tf_op jit(solution)/shard_map/while/body/eval_jaxpr/dot_general | solution.py:70
  252.4 3.6 %all-to-all-start.3 = ((bf16[16,384,64]{1,2,0:T(8,128)(2,1)}), bf16[16,384,64]{1,2,0:T(8,128)(2,1)S(1)}, u32[]{:S(2)}, u32[]{:S(2)}) async-start(bf16[16,384,64]{1,2,0:T(8,128)(2,1)} %copy.25), calls=%async_computation.3 | async-start | bytes 1572864 | tf_op jit(solution)/shard_map/all_to_all | solution.py:115
  256.0 12.0 %all-to-all-done.3 = bf16[16,384,64]{1,2,0:T(8,128)(2,1)S(1)} async-done(((bf16[16,384,64]{1,2,0:T(8,128)(2,1)}), bf16[16,384,64]{1,2,0:T(8,128)(2,1)S(1)}, u32[]{:S(2)}, u32[]{:S(2)}) %all-to-all-start.3) | async-done | bytes 786464 | tf_op jit(solution)/shard_map/all_to_all | solution.py:115
  268.0 5.2 %fusion.12 = bf16[1,384,2048]{2,1,0:T(8,128)(2,1)} fusion(bf16[384,1024]{0,1:T(8,128)(2,1)S(1)} %bitcast.67, bf16[1024,2048]{0,1:T(8,128)(2,1)} %all-gather.5.cloned.1.call-done), kind=kOutput, calls=%fused_computation.16 | convolution fusion | flops 1611399168 | bytes 6553600 | tf_op jit(solution)/shard_map/dot_general | solution.py:116
  (78 shorter events, 57.7 us)
Async XLA Ops:
  6.5 74.7 %copy-start = (bf16[1,384,2048]{2,1,0:T(8,128)(2,1)S(1)}, bf16[1,384,2048]{2,1,0:T(8,128)(2,1)}, u32[]{:S(2)}) copy-start(bf16[1,384,2048]{2,1,0:T(8,128)(2,1)} %param.9) | copy-start | bytes 4718596
  6.5 74.7 %all-gather.3.cloned.1.call-start = ((), (), s32[]{:S(2)}) async-start(), calls=%async_computation.4 | async-start | bytes 6340608 | tf_op jit(solution)/shard_map/all_gather | solution.py:18
  8.4 74.8 %copy-start.4 = (f32[64]{0:T(128)S(1)}, f32[64]{0:T(128)}, u32[]{:S(2)}) copy-start(f32[64]{0:T(128)} %param.15) | copy-start | bytes 772
  84.4 19.1 %all-to-all-start.1 = ((bf16[384,16,64]{0,2,1:T(8,128)(2,1)}), bf16[384,16,64]{0,2,1:T(8,128)(2,1)S(1)}, u32[]{:S(2)}, u32[]{:S(2)}) async-start(bf16[384,16,64]{0,2,1:T(8,128)(2,1)} %bitcast.11), calls=%async_computation.1 | async-start | bytes 1572864 | tf_op jit(solution)/shard_map/all_to_all | solution.py:111
  88.8 4.6 %copy-start.5 = (f32[64]{0:T(128)S(1)}, f32[64]{0:T(128)}, u32[]{:S(2)}) copy-start(f32[64]{0:T(128)} %param.14) | copy-start | bytes 772
  103.5 5.6 %copy-start.1 = (bf16[384,16,64]{0,2,1:T(8,128)(2,1)}, bf16[384,16,64]{0,2,1:T(8,128)(2,1)S(1)}, u32[]{:S(2)}) copy-start(bf16[384,16,64]{0,2,1:T(8,128)(2,1)S(1)} %all-to-all-done.1) | copy-start | bytes 2359300
  103.5 17.3 %all-to-all-start = ((bf16[384,16,64]{0,2,1:T(8,128)(2,1)}), bf16[384,16,64]{0,2,1:T(8,128)(2,1)S(1)}, u32[]{:S(2)}, u32[]{:S(2)}) async-start(bf16[384,16,64]{0,2,1:T(8,128)(2,1)} %pad_maximum_fusion), calls=%async_computation | async-start | bytes 1572864 | tf_op jit(solution)/shard_map/all_to_all | solution.py:108
  120.8 6.2 %copy-start.2 = (bf16[384,16,64]{0,2,1:T(8,128)(2,1)}, bf16[384,16,64]{0,2,1:T(8,128)(2,1)S(1)}, u32[]{:S(2)}) copy-start(bf16[384,16,64]{0,2,1:T(8,128)(2,1)S(1)} %all-to-all-done) | copy-start | bytes 2359300
  121.9 17.1 %all-to-all-start.2 = ((bf16[384,16,64]{0,2,1:T(8,128)(2,1)}), bf16[384,16,64]{0,2,1:T(8,128)(2,1)}, u32[]{:S(2)}, u32[]{:S(2)}) async-start(bf16[384,16,64]{0,2,1:T(8,128)(2,1)} %bitcast.16), calls=%async_computation.2 | async-start | bytes 1572864 | tf_op jit(solution)/shard_map/all_to_all | solution.py:112
  126.2 129.8 %all-gather.5.cloned.1.call-start = ((), (), s32[]{:S(2)}) async-start(), calls=%async_computation.5 | async-start | bytes 4227072 | tf_op jit(solution)/shard_map/all_gather | solution.py:118
  144.3 2.2 copy-start.3
  153.3 2.2 copy-start.3
  162.2 2.2 copy-start.3
  171.2 2.2 copy-start.3
  180.2 2.2 copy-start.3
  189.1 2.2 copy-start.3
  198.1 2.2 copy-start.3
  207.1 2.2 copy-start.3
  216.0 2.2 copy-start.3
  225.0 2.2 copy-start.3
  233.9 2.2 copy-start.3
  242.9 2.2 copy-start.3
  252.4 15.6 %all-to-all-start.3 = ((bf16[16,384,64]{1,2,0:T(8,128)(2,1)}), bf16[16,384,64]{1,2,0:T(8,128)(2,1)S(1)}, u32[]{:S(2)}, u32[]{:S(2)}) async-start(bf16[16,384,64]{1,2,0:T(8,128)(2,1)} %copy.25), calls=%async_computation.3 | async-start | bytes 1572864 | tf_op jit(solution)/shard_map/all_to_all | solution.py:115
Sparse Core Ops, SparseCore 0:
  10.4 70.7 all-gather.2
  130.1 66.7 all-gather.4
where the time goes:
time: 281 us; the launch traced here: 280 us
  waiting for transfers between devices  113 us (40%)
  matrix products  95 us (34%)
  other arithmetic  29.7 us (11%)
  starting transfers between devices  16.1 us (6%)
  between operations  13.6 us (5%)
  local copies, waits for them, and re-layouts  12.1 us (4%)
    all_gather x1, waiting for transfers between devices, in_one_piece(): filled = lax.all_gather(both, axis, axis=dim, tiled=True)  72.8 us
    dot_general x12, matrix products, attend_block(): jnp.dot(shares, value_rows, preferred_element_type=jnp.float32)  47.9 us
    dot_general x12, matrix products, attend_block(): lax.dot_general(segment, key_rows, (((1,), (1,)), ((), ())), preferred_el...  33.4 us
    reduce_sum x12, other arithmetic, attend_block(): jnp.sum(weights, axis=-1, keepdims=True)  26.2 us
    all_to_all x1, waiting for transfers between devices, per_device(): lax.all_to_all(outputs, 'sp', split_axis=0, concat_axis=1, tiled=True)  12 us
    all_to_all x1, waiting for transfers between devices, per_device(): lax.all_to_all(queries.reshape(tok_count, q_width), 'sp', split_axis=1, c...  11.7 us
    dot_general x3, matrix products, per_device(): jnp.dot(rows_in, rows_part, preferred_element_type=jnp.float32)  8.55 us
    all_to_all x1, waiting for transfers between devices, per_device(): lax.all_to_all(keys_wide, 'sp', split_axis=1, concat_axis=0, tiled=True)  8.52 us
  transfers between devices with their start and end apart: 6, of which 5 were waited for; matrix products, arithmetic and copies ran while one was open for 45% of the time, Pallas kernels for 0%

commit v1 on v0

--- a/solution.py
+++ b/solution.py
@@ -3,10 +3,13 @@
 import jax
 import jax.numpy as jnp
 from jax import lax
+from jax.experimental import pallas as pl
+from jax.experimental.pallas import tpu as pltpu
 from jax.sharding import PartitionSpec as P
 
 GRID_W = 64
-
+LOG2E = 1.4426950408889634
+V_ROWS = 80
 
 epsilon = 1e-06
 rope_base = 10000.0
@@ -52,25 +55,81 @@
     )
 
 
-def attend(query_rows, key_rows, value_rows):
-    row_count, head_width = query_rows.shape
-    block_rows = math.gcd(row_count, 512)
-    score_scale = head_width ** (-0.5)
+def _attend_call(kern, q_t, k2, v_t, q_block, name):
+    rows = q_t.shape[1]
+    keys = k2.shape[0]
+    return pl.pallas_call(
+        kern,
+        grid=(rows // q_block,),
+        in_specs=[
+            pl.BlockSpec((64, q_block), lambda i: (0, i)),
+            pl.BlockSpec((keys, 128), lambda i: (0, 0)),
+            pl.BlockSpec((V_ROWS, keys), lambda i: (0, 0)),
+        ],
+        out_specs=pl.BlockSpec((64, q_block), lambda i: (0, i)),
+        out_shape=jax.ShapeDtypeStruct((64, rows), jnp.bfloat16),
+        compiler_params=pltpu.CompilerParams(vmem_limit_bytes=56 * 2**20),
+        name=name,
+    )(q_t, k2, v_t)
 
-    def attend_block(segment):
-        scores = (
-            lax.dot_general(
-                segment, key_rows, (((1,), (1,)), ((), ())), preferred_element_type=jnp.float32
-            )
-            * score_scale
+
+def attend_bounded(q_t, k2, v_t):
+    key_tile = 1024
+
+    def kern(q_ref, k_ref, v_ref, o_ref):
+        scaled = q_ref[...].astype(jnp.float32) * (0.125 * LOG2E)
+        high = scaled.astype(jnp.bfloat16)
+        low = (scaled - high.astype(jnp.float32)).astype(jnp.bfloat16)
+        q2 = jnp.concatenate([high, low], axis=0)
+        acc = jnp.zeros((V_ROWS, q2.shape[1]), jnp.float32)
+        for u in range(k_ref.shape[0] // key_tile):
+            rows = pl.ds(u * key_tile, key_tile)
+            scores = jnp.dot(k_ref[rows, :], q2, preferred_element_type=jnp.float32)
+            weights = jnp.exp2(scores).astype(jnp.bfloat16)
+            acc = acc + jnp.dot(v_ref[:, rows], weights, preferred_element_type=jnp.float32)
+        o_ref[...] = (acc[:64] / acc[64:65]).astype(jnp.bfloat16)
+
+    return _attend_call(kern, q_t, k2, v_t, 1024, "attend_bounded")
+
+
+def attend_running_max(q_t, k2, v_t):
+    key_tile = 512
+
+    def kern(q_ref, k_ref, v_ref, o_ref):
+        q = q_ref[...]
+
+        def step(u, carry):
+            top, acc = carry
+            rows = pl.ds(pl.multiple_of(u * key_tile, key_tile), key_tile)
+            scores = jnp.dot(k_ref[rows, :64], q, preferred_element_type=jnp.float32) * 0.125
+            new_top = jnp.maximum(top, jnp.max(scores, axis=0, keepdims=True))
+            weights = jnp.exp(scores - new_top).astype(jnp.bfloat16)
+            part = jnp.dot(v_ref[:, rows], weights, preferred_element_type=jnp.float32)
+            return new_top, acc * jnp.exp(top - new_top) + part
+
+        start = (
+            jnp.full((1, q.shape[1]), -1e30, jnp.float32),
+            jnp.zeros((V_ROWS, q.shape[1]), jnp.float32),
         )
-        row_max = jnp.max(scores, axis=-1, keepdims=True)
-        weights = jnp.exp(scores - row_max)
-        shares = (weights / jnp.sum(weights, axis=-1, keepdims=True)).astype(jnp.bfloat16)
-        return jnp.dot(shares, value_rows, preferred_element_type=jnp.float32).astype(jnp.bfloat16)
+        _, acc = lax.fori_loop(0, k_ref.shape[0] // key_tile, step, start)
+        o_ref[...] = (acc[:64] / acc[64:65]).astype(jnp.bfloat16)
 
-    blocks = query_rows.reshape(row_count // block_rows, block_rows, head_width)
-    return lax.map(attend_block, blocks).reshape(row_count, head_width)
+    return _attend_call(kern, q_t, k2, v_t, 512, "attend_running_max")
+
+
+def attend(query_rows, key_rows, value_rows, bounded):
+    keys = key_rows.shape[0]
+    q_t = query_rows.T
+    k2 = jnp.concatenate([key_rows, key_rows], axis=1)
+    v_t = jnp.concatenate(
+        [
+            value_rows.T,
+            jnp.ones((1, keys), jnp.bfloat16),
+            jnp.zeros((V_ROWS - 65, keys), jnp.bfloat16),
+        ],
+        axis=0,
+    )
+    return lax.cond(bounded, attend_bounded, attend_running_max, q_t, k2, v_t).T
 
 
 def per_device(tokens, q_weight, k_weight, v_weight, out_weight, q_gain, k_gain):
@@ -83,6 +142,7 @@
     kv_heads = kv_width // head_width
     group_size = q_heads // kv_heads
     offset = lax.axis_index("sp") * tok_count
+    bounded = 8.0 * jnp.max(jnp.abs(q_gain)) * jnp.max(jnp.abs(k_gain)) <= 60.0
     weight_rows = in_one_piece((q_weight, k_weight, v_weight), ("sp", "dp"), 0, 1)
     query_raw, key_raw, value_raw = tuple(
         (
@@ -111,7 +171,7 @@
         lax.all_to_all(keys_wide, "sp", split_axis=1, concat_axis=0, tiled=True),
         lax.all_to_all(values_wide, "sp", split_axis=1, concat_axis=0, tiled=True),
     )
-    outputs = attend(q_local, k_local, v_local)
+    outputs = attend(q_local, k_local, v_local, bounded)
     attended = lax.all_to_all(outputs, "sp", split_axis=0, concat_axis=1, tiled=True)
     result = jnp.dot(
         attended,

time: 281 us -> 267 us (0.950)
  Pallas kernels: 0 us -> 89.6 us
  matrix products: 95 us -> 13.7 us
  other arithmetic: 29.7 us -> 6.13 us
  waiting for transfers between devices: 113 us -> 118 us
  local copies, waits for them, and re-layouts: 12.1 us -> 8.08 us
    pallas_call x0 -> x1, Pallas kernels: none -> 89.6 us  [_attend_call(): pl.pallas_call(kern, grid=(rows // q_block,), in_specs=[pl.BlockSpec((64,...]
    dot_general x24 -> x0, matrix products: 81.3 us -> none  [the longest x12 47.9 us: attend_block(): jnp.dot(shares, value_rows, preferred_element_type=jnp.float32)]
    reduce_sum x12 -> x0, other arithmetic: 26.2 us -> none  [attend_block(): jnp.sum(weights, axis=-1, keepdims=True)]
    while x27 -> x0, local copies, waits for them, and re-layouts: 5.87 us -> none  [the longest x3 5.83 us: attend(): return lax.map(attend_block, blocks).reshape(row_count, head_width)]
    all_to_all x1, waiting for transfers between devices: 8.52 us -> 12.2 us  [per_device(): lax.all_to_all(keys_wide, 'sp', split_axis=1, concat_axis=0, tiled=True)]
  transfers between devices with their start and end apart: 6 -> 6, of which waited for: 5 -> 5; matrix products, arithmetic and copies ran while one was open for 45% -> 8% of each run, Pallas kernels for 0% -> 34%
where the time goes in v1:
time: 267 us
  waiting for transfers between devices  118 us (44%)
  Pallas kernels  89.6 us (34%)
  starting transfers between devices  15.9 us (6%)
  between operations  14.9 us (6%)
  matrix products  13.7 us (5%)
  local copies, waits for them, and re-layouts  8.08 us (3%)
  other arithmetic  6.13 us (2%)
    pallas_call x1, Pallas kernels, _attend_call(): pl.pallas_call(kern, grid=(rows // q_block,), in_specs=[pl.BlockSpec((64,...  89.6 us
    all_gather x1, waiting for transfers between devices, in_one_piece(): filled = lax.all_gather(both, axis, axis=dim, tiled=True)  72 us
    all_to_all x1, waiting for transfers between devices, per_device(): lax.all_to_all(queries.reshape(tok_count, q_width), 'sp', split_axis=1, c...  12.7 us
    all_to_all x1, waiting for transfers between devices, per_device(): lax.all_to_all(keys_wide, 'sp', split_axis=1, concat_axis=0, tiled=True)  12.2 us
    all_to_all x1, waiting for transfers between devices, per_device(): lax.all_to_all(outputs, 'sp', split_axis=0, concat_axis=1, tiled=True)  11.5 us
    all_to_all x1, waiting for transfers between devices, per_device(): lax.all_to_all(values_wide, 'sp', split_axis=1, concat_axis=0, tiled=True)  8.95 us
    dot_general x3, matrix products, per_device(): jnp.dot(rows_in, rows_part, preferred_element_type=jnp.float32)  8.56 us
  transfers between devices with their start and end apart: 6, of which 5 were waited for; matrix products, arithmetic and copies ran while one was open for 8% of the time, Pallas kernels for 34%

profile of v1, /device:TPU:0, one launch (start us, length us, event | category | flops | bytes accessed | tf_op | source)
XLA Modules:
  0.0 266.8 jit_solution(15671406487255541625)
XLA Ops:
  6.5 1.5 pad_maximum_fusion.3
  8.1 0.7 all-gather.5.cloned.1.call-update
  8.9 0.3 multiply_cosine_fusion.1
  9.2 72.0 %all-gather.3.cloned.1.call-done = bf16[2048,1536]{1,0:T(8,128)(2,1)} async-done(((bf16[16,1536]{1,0:T(8,128)(2,1)}), bf16[2048,1536]{1,0:T(8,128)(2,1)}) %all-gather.3.cloned.1.call-update) | async-done | bytes 6291472 | tf_op jit(solution)/shard_map/all_gather | solution.py:21
  81.2 4.6 %multiply_reduce_fusion = (f32[384,16]{0,1:T(8,128)S(1)}, f32[1024,384]{1,0:T(8,128)S(1)}) fusion(bf16[1,384,2048]{2,1,0:T(8,128)(2,1)S(1)} %copy-done, bf16[2048,1536]{1,0:T(8,128)(2,1)} %all-gather.3.cloned.1.call-done), kind=kOutput, calls=%fused_computation.11 | convolution fusion | flops 1611393024 | bytes 7364608 | tf_op jit(solution)/shard_map/dot_general | solution.py:149
  85.8 0.3 multiply_multiply_fusion
  86.2 0.2 subtract_convert_fusion.1
  86.4 1.0 pad_maximum_fusion.1
  87.4 4.4 %all-to-all-start = ((bf16[384,16,64]{0,2,1:T(8,128)(2,1)}), bf16[384,16,64]{0,2,1:T(8,128)(2,1)S(1)}, u32[]{:S(2)}, u32[]{:S(2)}) async-start(bf16[384,16,64]{0,2,1:T(8,128)(2,1)} %pad_maximum_fusion.1), calls=%async_computation | async-start | bytes 1572864 | tf_op jit(solution)/shard_map/all_to_all | solution.py:168
  91.8 2.0 multiply_reduce_fusion.1
  94.0 12.7 %all-to-all-done = bf16[384,16,64]{0,2,1:T(8,128)(2,1)S(1)} async-done(((bf16[384,16,64]{0,2,1:T(8,128)(2,1)}), bf16[384,16,64]{0,2,1:T(8,128)(2,1)S(1)}, u32[]{:S(2)}, u32[]{:S(2)}) %all-to-all-start) | async-done | bytes 786464 | tf_op jit(solution)/shard_map/all_to_all | solution.py:168
  106.7 1.0 broadcast_in_dim.12
  107.7 3.6 %all-to-all-start.1 = ((bf16[384,16,64]{0,2,1:T(8,128)(2,1)}), bf16[384,16,64]{0,2,1:T(8,128)(2,1)S(1)}, u32[]{:S(2)}, u32[]{:S(2)}) async-start(bf16[384,16,64]{0,2,1:T(8,128)(2,1)} %bitcast.61), calls=%async_computation.1 | async-start | bytes 1572864 | tf_op jit(solution)/shard_map/all_to_all | solution.py:171
  111.3 2.0 fusion.8
  113.3 12.2 %all-to-all-done.1 = bf16[384,16,64]{0,2,1:T(8,128)(2,1)S(1)} async-done(((bf16[384,16,64]{0,2,1:T(8,128)(2,1)}), bf16[384,16,64]{0,2,1:T(8,128)(2,1)S(1)}, u32[]{:S(2)}, u32[]{:S(2)}) %all-to-all-start.1) | async-done | bytes 786464 | tf_op jit(solution)/shard_map/all_to_all | solution.py:171
  125.6 1.0 broadcast_in_dim.14
  126.6 4.3 %all-to-all-start.2 = ((bf16[384,16,64]{0,2,1:T(8,128)(2,1)}), bf16[384,16,64]{0,2,1:T(8,128)(2,1)}, u32[]{:S(2)}, u32[]{:S(2)}) async-start(bf16[384,16,64]{0,2,1:T(8,128)(2,1)} %bitcast.59), calls=%async_computation.2 | async-start | bytes 1572864 | tf_op jit(solution)/shard_map/all_to_all | solution.py:172
  130.9 0.6 abs_reduce_fusion.1
  132.1 0.6 abs_reduce_fusion
  133.5 1.0 copy.27
  134.5 1.0 copy.28
  135.5 8.9 %all-to-all-done.2 = bf16[384,16,64]{0,2,1:T(8,128)(2,1)} async-done(((bf16[384,16,64]{0,2,1:T(8,128)(2,1)}), bf16[384,16,64]{0,2,1:T(8,128)(2,1)}, u32[]{:S(2)}, u32[]{:S(2)}) %all-to-all-start.2) | async-done | bytes 786464 | tf_op jit(solution)/shard_map/all_to_all | solution.py:172
  144.5 1.3 copy.29
  145.9 0.1 pad_maximum_fusion
  146.0 1.2 maximum_maximum_fusion
  147.2 91.4 %conditional.1 = (bf16[64,6144]{1,0:T(8,128)(2,1)S(1)}) conditional(s32[]{:T(128)} %convert_element_type.36, (bf16[64,6144]{1,0:T(8,128)(2,1)}, bf16[6144,128]{0,1:T(8,128)(2,1)S(1)}, bf16[80,6144]{1,0:T(8,128)(2,1)}) %tuple.35, (bf16[64,6144]{1,0:T(8,128)(2,1)}, bf16[6144,128]{0,1:T(8,128)(2,1)S(1)}, bf16[80,6144]{1,0:T(8,128)(2,1)}) %tuple.36), branch_computations={%region_4.5_spmd, %region_5.6_spmd} | conditional | bytes 3145736 | solution.py:132
  147.2 1.6 copy.23.k_ref
  148.8 89.6 %attend_running_max.1 = bf16[64,6144]{1,0:T(8,128)(2,1)S(1)} custom-call(bf16[64,6144]{1,0:T(8,128)(2,1)} %get-tuple-element.20.q_ref, bf16[6144,128]{1,0:T(8,128)(2,1)} %copy.23.k_ref, bf16[80,6144]{1,0:T(8,128)(2,1)} %get-tuple-element.22.v_ref), custom_call_target="tpu_custom_call" | custom-call | tf_op jit(solution)/shard_map/cond/branch_0_fun/attend_running_max/pallas_call | solution.py:61
  238.6 1.0 copy.31
  239.6 3.6 %all-to-all-start.3 = ((bf16[16,384,64]{1,2,0:T(8,128)(2,1)}), bf16[16,384,64]{1,2,0:T(8,128)(2,1)S(1)}, u32[]{:S(2)}, u32[]{:S(2)}) async-start(bf16[16,384,64]{1,2,0:T(8,128)(2,1)} %bitcast.53), calls=%async_computation.3 | async-start | bytes 1572864 | tf_op jit(solution)/shard_map/all_to_all | solution.py:175
  243.3 11.5 %all-to-all-done.3 = bf16[16,384,64]{1,2,0:T(8,128)(2,1)S(1)} async-done(((bf16[16,384,64]{1,2,0:T(8,128)(2,1)}), bf16[16,384,64]{1,2,0:T(8,128)(2,1)S(1)}, u32[]{:S(2)}, u32[]{:S(2)}) %all-to-all-start.3) | async-done | bytes 786464 | tf_op jit(solution)/shard_map/all_to_all | solution.py:175
  254.8 5.2 %fusion.2 = bf16[1,384,2048]{2,1,0:T(8,128)(2,1)} fusion(bf16[384,1024]{0,1:T(8,128)(2,1)S(1)} %bitcast.63, bf16[1024,2048]{0,1:T(8,128)(2,1)} %all-gather.5.cloned.1.call-done), kind=kOutput, calls=%fused_computation.3 | convolution fusion | flops 1611399168 | bytes 6553600 | tf_op jit(solution)/shard_map/dot_general | solution.py:176
  (22 shorter events, 0.6 us)
Async XLA Ops:
  6.5 74.7 %copy-start = (bf16[1,384,2048]{2,1,0:T(8,128)(2,1)S(1)}, bf16[1,384,2048]{2,1,0:T(8,128)(2,1)}, u32[]{:S(2)}) copy-start(bf16[1,384,2048]{2,1,0:T(8,128)(2,1)} %param.9) | copy-start | bytes 4718596
  6.5 74.7 %all-gather.3.cloned.1.call-start = ((), (), s32[]{:S(2)}) async-start(), calls=%async_computation.4 | async-start | bytes 6340608 | tf_op jit(solution)/shard_map/all_gather | solution.py:21
  8.1 235.2 %all-gather.5.cloned.1.call-start = ((), (), s32[]{:S(2)}) async-start(), calls=%async_computation.5 | async-start | bytes 4227072 | tf_op jit(solution)/shard_map/all_gather | solution.py:178
  9.1 76.7 %copy-start.3 = (f32[64]{0:T(128)S(1)}, f32[64]{0:T(128)}, u32[]{:S(2)}) copy-start(f32[64]{0:T(128)} %param.14) | copy-start | bytes 772
  87.4 19.3 %all-to-all-start = ((bf16[384,16,64]{0,2,1:T(8,128)(2,1)}), bf16[384,16,64]{0,2,1:T(8,128)(2,1)S(1)}, u32[]{:S(2)}, u32[]{:S(2)}) async-start(bf16[384,16,64]{0,2,1:T(8,128)(2,1)} %pad_maximum_fusion.1), calls=%async_computation | async-start | bytes 1572864 | tf_op jit(solution)/shard_map/all_to_all | solution.py:168
  91.8 2.0 copy-start.2
  107.7 17.8 %all-to-all-start.1 = ((bf16[384,16,64]{0,2,1:T(8,128)(2,1)}), bf16[384,16,64]{0,2,1:T(8,128)(2,1)S(1)}, u32[]{:S(2)}, u32[]{:S(2)}) async-start(bf16[384,16,64]{0,2,1:T(8,128)(2,1)} %bitcast.61), calls=%async_computation.1 | async-start | bytes 1572864 | tf_op jit(solution)/shard_map/all_to_all | solution.py:171
  126.6 17.9 %all-to-all-start.2 = ((bf16[384,16,64]{0,2,1:T(8,128)(2,1)}), bf16[384,16,64]{0,2,1:T(8,128)(2,1)}, u32[]{:S(2)}, u32[]{:S(2)}) async-start(bf16[384,16,64]{0,2,1:T(8,128)(2,1)} %bitcast.59), calls=%async_computation.2 | async-start | bytes 1572864 | tf_op jit(solution)/shard_map/all_to_all | solution.py:172
  144.5 1.4 copy-start.1
  239.6 15.2 %all-to-all-start.3 = ((bf16[16,384,64]{1,2,0:T(8,128)(2,1)}), bf16[16,384,64]{1,2,0:T(8,128)(2,1)S(1)}, u32[]{:S(2)}, u32[]{:S(2)}) async-start(bf16[16,384,64]{1,2,0:T(8,128)(2,1)} %bitcast.53), calls=%async_computation.3 | async-start | bytes 1572864 | tf_op jit(solution)/shard_map/all_to_all | solution.py:175
Sparse Core Ops, SparseCore 0:
  10.4 70.7 all-gather.2
  84.3 69.4 all-gather.4
